TPU v7x, 32 devices: a whole 2x2x4 slice. The times are simulated.
32 devices in a mesh: ep: 8 (over z, y), tp: 4 (over x, core).
Axes of the slice: x: 2, y: 2, z: 4, core: 2. Of those that a mesh axis runs over, the one named last changes fastest.
Arguments:
- c_gate: bfloat16 [2048, 1024], P('ep', 'tp'), may hold values from -6 to 6
- b_gate: bfloat16 [2048, 1024], P('ep', 'tp'), may hold values from -6 to 6
- values: bfloat16 [2048, 1024], P('ep', 'tp'), may hold values from -6 to 6
- conv_taps: float32 [3, 1024], P(None, 'tp'), may hold values from -3.5 to 3.5
- w_mix_out: bfloat16 [1024, 2048], P('tp'), may hold values from -0.1875 to 0.1875
- moe_in: bfloat16 [4096, 2048], P(('ep', 'tp')), may hold values from -6 to 6
- norm_gain: float32 [2048], replicated, may hold values from 0.1 to 1.9
- route_ids: int32 [4096, 2], P(('ep', 'tp')), may hold values from 0 to 7, all different within a row; in each aligned block of 128 rows (0 to 127, 128 to 255, ...) at most 40 rows name the same one
- route_weights: float32 [4096, 2], P(('ep', 'tp')), may hold values from 0.1 to 1
- w_gate: bfloat16 [8, 2048, 3584], P('ep', None, 'tp'), may hold values from -0.125 to 0.125
- w_up: bfloat16 [8, 2048, 3584], P('ep', None, 'tp'), may hold values from -0.125 to 0.125
- w_down: bfloat16 [8, 3584, 2048], P('ep', 'tp'), may hold values from -0.09375 to 0.09375
Outputs:
- mixer_out: bfloat16 [2048, 2048], P(('ep', 'tp'))
- moe_out: bfloat16 [4096, 2048], P(('ep', 'tp'))
Inputs may be any that keep to these rules, and one draw needn't show every extreme that they name: `route_ids`: each row names 2 different experts; in each aligned block of 128 rows (the rows of one device) no expert is named by more than 40 rows, and in every draw some expert is named by exactly 40 rows in some block.
All inputs are finite; a program needn't handle non-finite values.
Results may differ from a plain program's by a relative error of at most 0.012.
Values may be sent and summed in bfloat16 or wider, within the bound.
A program may use at most 128 MiB of HBM per device.

v0:
```python
import jax
import jax.numpy as jnp
from jax import lax
from jax.sharding import PartitionSpec as P

EPS = 1e-06


def passed_along(block, axis, distance):
    devices = range(lax.axis_size(axis))
    route = [(i - distance, i) for i in devices if i - distance in devices]
    return lax.ppermute(block, axis, route)


def rank_copies(route_block, experts):
    flat_ids = route_block.reshape(-1)
    onehot = (flat_ids[:, None] == jnp.arange(experts, dtype=jnp.int32)[None, :]).astype(jnp.int32)
    before = jnp.cumsum(onehot, axis=0) - onehot
    return (flat_ids, jnp.sum(before * onehot, axis=1))


def pack_rows(rows, slot_of, top, slot_count):
    copies = slot_of.shape[0]
    table = (
        jnp.full((slot_count,), copies, jnp.int32)
        .at[slot_of]
        .set(jnp.arange(copies, dtype=jnp.int32))
    )
    padded = jnp.concatenate([rows, jnp.zeros((1, rows.shape[1]), rows.dtype)], 0)
    return padded[table // top]


def on_device(
    c_gate,
    b_gate,
    values,
    conv_taps,
    w_mix_out,
    moe_in,
    norm_gain,
    route_ids,
    route_weights,
    w_gate,
    w_up,
    w_down,
):
    tokens = c_gate.shape[0]
    reach = conv_taps.shape[0] - 1
    product = c_gate.astype(jnp.float32) * values.astype(jnp.float32)
    previous = passed_along(product[tokens - reach :], "ep", 1)
    extended = jnp.concatenate([previous, product], 0)
    convolved = jnp.zeros_like(product)
    for offset in range(reach + 1):
        convolved = convolved + conv_taps[offset][None, :] * extended[offset : offset + tokens]
    mixed = (b_gate.astype(jnp.float32) * convolved).astype(jnp.bfloat16)
    piece = mixed
    mixer_out = lax.psum_scatter(
        jnp.dot(piece, w_mix_out, preferred_element_type=jnp.float32).astype(jnp.bfloat16),
        "tp",
        scatter_dimension=0,
        tiled=True,
    )
    rows_b = moe_in.shape[0]
    width = moe_in.shape[1]
    top = route_ids.shape[1]
    n_ep = lax.axis_size("ep")
    experts = w_gate.shape[0] * n_ep
    capacity = 5 * rows_b * top // (4 * experts)
    stream = moe_in.astype(jnp.float32)
    scale = lax.rsqrt(jnp.mean(stream * stream, axis=1, keepdims=True) + EPS)
    normed = (stream * scale * norm_gain[None, :]).astype(jnp.bfloat16)
    own_ids, own_ranks = rank_copies(route_ids, experts)
    own_slot = own_ids * capacity + own_ranks
    outgoing = pack_rows(normed, own_slot, top, experts * capacity).reshape(
        experts, capacity, width
    )
    arrived = lax.all_to_all(outgoing, "ep", split_axis=0, concat_axis=1, tiled=True).reshape(
        -1, width
    )
    piece = lax.all_gather(arrived, "tp", axis=0, tiled=True)
    gate_val = jnp.dot(piece, w_gate[0], preferred_element_type=jnp.float32)
    up_val = jnp.dot(piece, w_up[0], preferred_element_type=jnp.float32)
    hidden = (jax.nn.silu(gate_val) * up_val).astype(jnp.bfloat16)
    piece = hidden
    expert_out = lax.psum_scatter(
        jnp.dot(piece, w_down[0], preferred_element_type=jnp.float32).astype(jnp.bfloat16),
        "tp",
        scatter_dimension=0,
        tiled=True,
    )
    returned = lax.all_to_all(
        expert_out.reshape(n_ep, capacity, width), "ep", split_axis=0, concat_axis=0, tiled=True
    )
    picked = returned.reshape(-1, width)[own_slot].astype(jnp.float32).reshape(rows_b, top, width)
    moe_out = jnp.sum(picked * route_weights[:, :, None], axis=1).astype(jnp.bfloat16)
    return (mixer_out, moe_out)


def solution(mesh):
    return jax.shard_map(
        on_device,
        mesh=mesh,
        in_specs=(
            P("ep", "tp"),
            P("ep", "tp"),
            P("ep", "tp"),
            P(None, "tp"),
            P("tp", None),
            P(("ep", "tp"), None),
            P(),
            P(("ep", "tp"), None),
            P(("ep", "tp"), None),
            P("ep", None, "tp"),
            P("ep", None, "tp"),
            P("ep", "tp", None),
        ),
        out_specs=(P(("ep", "tp"), None), P(("ep", "tp"), None)),
        check_vma=False,
    )
```

profile of v0, /device:TPU:0, one launch (start us, length us, event | category | flops | bytes accessed | tf_op | source)
XLA Modules:
  0.0 225.9 jit_solution(5332753036802523370)
XLA Ops:
  7.2 0.9 copy.16
  8.2 0.1 eq.25
  8.4 0.7 broadcast_multiply_fusion
  9.1 0.6 reduce-window.6
  9.6 0.2 slice_reduce_fusion
  10.0 0.1 mul.107
  10.3 1.4 scatter_custom_fusion
  11.7 1.2 fusion.4
  12.9 1.2 fusion.6
  14.2 2.4 %gather_fusion = bf16[320,2048]{1,0:T(8,128)(2,1)S(1)} fusion(bf16[129,2048]{1,0:T(8,128)(2,1)S(1)} %concatenate.7, s32[1024]{0:T(1024)S(1)} %pad_clamp_fusion.1), kind=kCustom, calls=%fused_computation | custom fusion | bytes 2622720 | tf_op jit(solution)/shard_map/gather | solution.py:30
  16.7 38.6 %all_to_all.14 = bf16[8,40,2048]{2,1,0:T(8,128)(2,1)} all-to-all(bf16[8,40,2048]{2,1,0:T(8,128)(2,1)S(1)} %bitcast.39), channel_id=1, replica_groups=mesh['ep'=8,'tp'=4] {'ep'}, dimensions={0} | all-to-all | bytes 2621440 | tf_op jit(solution)/shard_map/all_to_all | solution.py:77
  55.3 39.5 %all-gather.2.cloned.1.call-done = bf16[1280,2048]{1,0:T(8,128)(2,1)} async-done(((bf16[320,2048]{1,0:T(8,128)(2,1)}), bf16[1280,2048]{1,0:T(8,128)(2,1)}) %all-gather.2.cloned.1.call-update) | async-done | bytes 5242896 | tf_op jit(solution)/shard_map/all_gather | solution.py:80
  94.9 10.0 %fusion.2 = f32[1280,896]{1,0:T(8,128)} fusion(bf16[1280,2048]{1,0:T(8,128)(2,1)} %all-gather.2.cloned.1.call-done, bf16[1,2048,896]{2,1,0:T(8,128)(2,1)} %param.21), kind=kOutput, calls=%fused_computation.7 | convolution fusion | flops 4697620480 | bytes 13500416 | tf_op jit(solution)/shard_map/dot_general | solution.py:81
  104.8 17.6 %convolution_convert_fusion = bf16[1280,2048]{1,0:T(8,128)(2,1)} fusion(bf16[1,896,2048]{2,1,0:T(8,128)(2,1)} %param.23, f32[1280,896]{1,0:T(8,128)} %fusion.2, bf16[1280,2048]{1,0:T(8,128)(2,1)} %all-gather.2.cloned.1.call-done, bf16[1,2048,896]{2,1,0:T(8,128)(2,1)} %param.22), kind=kOutput, calls=%fused_computation.3 | convolution fusion | flops 9404743680 | bytes 22413312 | tf_op jit(solution)/shard_map/dot_general | solution.py:86
  122.4 0.9 copy-done.2
  123.4 3.4 %collective-permute-start = (f32[2,256]{1,0:T(2,128)S(1)}, f32[2,256]{1,0:T(2,128)S(1)}, u32[]{:S(2)}, u32[]{:S(2)}) collective-permute-start(f32[2,256]{1,0:T(2,128)S(1)} %slice.36), channel_id=1, source_target_pairs={{0,4},{4,8},{8,12},{12,16},{16,20},{20,24},{24,28},{1,5},{5,9},{9,... | collective-permute-start | bytes 6152 | tf_op jit(solution)/shard_map/ppermute | solution.py:12
  126.8 47.2 %reduce-scatter.5.cloned.1.call-done = bf16[320,2048]{1,0:T(8,128)(2,1)} async-done(((bf16[1280,2048]{1,0:T(8,128)(2,1)}), bf16[320,2048]{1,0:T(8,128)(2,1)}) %reduce-scatter.5.cloned.1.call-update) | async-done | bytes 1310736 | tf_op jit(solution)/shard_map/reduce_scatter | solution.py:85
  174.0 5.5 %all-to-all-start.1 = ((bf16[8,40,2048]{2,1,0:T(8,128)(2,1)}), bf16[8,40,2048]{2,1,0:T(8,128)(2,1)S(1)}, u32[]{:S(2)}, u32[]{:S(2)}) async-start(bf16[8,40,2048]{2,1,0:T(8,128)(2,1)} %bitcast.41), calls=%async_computation.3 | async-start | bytes 2621440 | tf_op jit(solution)/shard_map/all_to_all | solution.py:91
  179.5 0.2 reduce-scatter.3.cloned.1.call-start
  179.8 1.5 convolution_convert_fusion.1
  181.4 29.3 %all-to-all-done.1 = bf16[8,40,2048]{2,1,0:T(8,128)(2,1)S(1)} async-done(((bf16[8,40,2048]{2,1,0:T(8,128)(2,1)}), bf16[8,40,2048]{2,1,0:T(8,128)(2,1)S(1)}, u32[]{:S(2)}, u32[]{:S(2)}) %all-to-all-start.1) | async-done | bytes 1310752 | tf_op jit(solution)/shard_map/all_to_all | solution.py:91
  210.7 2.3 %gather_fusion.1 = bf16[256,2048]{1,0:T(8,128)(2,1)} fusion(bf16[320,2048]{1,0:T(8,128)(2,1)S(1)} %bitcast.38, s32[1024]{0:T(1024)S(1)} %pad_clamp_fusion), kind=kCustom, calls=%fused_computation.1 | custom fusion | bytes 2098176 | tf_op jit(solution)/shard_map/gather | solution.py:94
  213.0 2.4 %reshape.85 = f32[128,2,2048]{2,1,0:T(2,128)S(1)} reshape(bf16[256,2048]{1,0:T(8,128)(2,1)} %gather_fusion.1) | data formatting | bytes 3145728 | tf_op jit(solution)/shard_map/convert_element_type | solution.py:94
  215.4 3.9 %multiply_reduce_fusion = bf16[128,2048]{1,0:T(8,128)(2,1)} fusion(f32[128,2,2048]{2,1,0:T(2,128)S(1)} %reshape.85, f32[128,2]{1,0:T(8,128)S(1)} %copy.18), kind=kLoop, calls=%fused_computation.10 | loop fusion | flops 786432 | bytes 2622464 | tf_op jit(solution)/shard_map/reduce_sum | solution.py:95
  (35 shorter events, 0.8 us)
Async XLA Ops:
  7.2 172.6 %copy-start = (bf16[256,2048]{1,0:T(8,128)(2,1)S(1)}, bf16[256,2048]{1,0:T(8,128)(2,1)}, u32[]{:S(2)}) copy-start(bf16[256,2048]{1,0:T(8,128)(2,1)} %param.16) | copy-start | bytes 3145732
  7.2 87.7 %all-gather.2.cloned.1.call-start = ((), (), s32[]{:S(2)}) async-start(), calls=%async_computation.5 | async-start | bytes 6553600 | tf_op jit(solution)/shard_map/all_gather | solution.py:80
  55.3 118.7 %reduce-scatter.5.cloned.1.call-start = ((), (), s32[]{:S(2)}) async-start(), calls=%async_computation.6 | async-start | bytes 6553600 | tf_op jit(solution)/shard_map/reduce_scatter | solution.py:85
  122.4 0.9 copy-start.2
  122.4 1.0 copy-start.3
  122.4 57.3 %copy-start.4 = (f32[3,256]{1,0:T(4,128)S(1)}, f32[3,256]{1,0:T(4,128)}, u32[]{:S(2)}) copy-start(f32[3,256]{1,0:T(4,128)} %param.15) | copy-start | bytes 9220
  122.4 57.3 %copy-start.1 = (bf16[256,256]{1,0:T(8,128)(2,1)S(1)}, bf16[256,256]{1,0:T(8,128)(2,1)}, u32[]{:S(2)}) copy-start(bf16[256,256]{1,0:T(8,128)(2,1)} %param.13) | copy-start | bytes 393220
  123.4 57.9 %copy-start.5 = (f32[128,2]{0,1:T(2,128)S(1)}, f32[128,2]{0,1:T(2,128)}, u32[]{:S(2)}) copy-start(f32[128,2]{0,1:T(2,128)} %param.20) | copy-start | bytes 3076
  123.4 56.3 %collective-permute-start = (f32[2,256]{1,0:T(2,128)S(1)}, f32[2,256]{1,0:T(2,128)S(1)}, u32[]{:S(2)}, u32[]{:S(2)}) collective-permute-start(f32[2,256]{1,0:T(2,128)S(1)} %slice.36), channel_id=1, source_target_pairs={{0,4},{4,8},{8,12},{12,16},{16,20},{20,24},{24,28},{1,5},{5,9},{9,... | collective-permute-start | bytes 6152 | tf_op jit(solution)/shard_map/ppermute | solution.py:12
  174.0 36.7 %all-to-all-start.1 = ((bf16[8,40,2048]{2,1,0:T(8,128)(2,1)}), bf16[8,40,2048]{2,1,0:T(8,128)(2,1)S(1)}, u32[]{:S(2)}, u32[]{:S(2)}) async-start(bf16[8,40,2048]{2,1,0:T(8,128)(2,1)} %bitcast.41), calls=%async_computation.3 | async-start | bytes 2621440 | tf_op jit(solution)/shard_map/all_to_all | solution.py:91
  179.5 39.9 %reduce-scatter.3.cloned.1.call-start = ((), (), s32[]{:S(2)}) async-start(), calls=%async_computation.4 | async-start | bytes 1310720 | tf_op jit(solution)/shard_map/reduce_scatter | solution.py:57
Sparse Core Ops, SparseCore 0:
  55.4 39.4 all-gather.1
  122.6 51.3 reduce-scatter.4
  183.4 25.2 reduce-scatter.2
where the time goes:
time: 226 us
  waiting for transfers between devices  116 us (51%)
  blocking collectives  38.6 us (17%)
  matrix products  29 us (13%)
  between operations  13.9 us (6%)
  local copies, waits for them, and re-layouts  11.3 us (5%)
  starting transfers between devices  9.19 us (4%)
  other arithmetic  7.85 us (3%)
    reduce_scatter x1, waiting for transfers between devices, on_device(): lax.psum_scatter(jnp.dot(piece, w_down[0], preferred_element_type=jnp.flo...  47.2 us
    all_gather x1, waiting for transfers between devices, on_device(): piece = lax.all_gather(arrived, 'tp', axis=0, tiled=True)  39.5 us
    all_to_all x1, blocking collectives, on_device(): lax.all_to_all(outgoing, 'ep', split_axis=0, concat_axis=1, tiled=True)  38.6 us
    all_to_all x1, waiting for transfers between devices, on_device(): lax.all_to_all(expert_out.reshape(n_ep, capacity, width), 'ep', split_axi...  29.3 us
    dot_general x1, matrix products, on_device(): jnp.dot(piece, w_down[0], preferred_element_type=jnp.float32)  17.6 us
    dot_general x1, matrix products, on_device(): gate_val = jnp.dot(piece, w_gate[0], preferred_element_type=jnp.float32)  9.98 us
    all_to_all x1, starting transfers between devices, on_device(): lax.all_to_all(expert_out.reshape(n_ep, capacity, width), 'ep', split_axi...  5.52 us
  transfers between devices with their start and end apart: 5, of which 3 were waited for; matrix products, arithmetic and copies ran while one was open for 5% of the time, Pallas kernels for 0%

commit v1 on v0

--- a/solution.py
+++ b/solution.py
@@ -77,7 +77,12 @@
     arrived = lax.all_to_all(outgoing, "ep", split_axis=0, concat_axis=1, tiled=True).reshape(
         -1, width
     )
-    piece = lax.all_gather(arrived, "tp", axis=0, tiled=True)
+    ring = [arrived]
+    for hop in range(3):
+        ring.append(lax.ppermute(ring[-1], "tp", [(dev, (dev + 1) % 4) for dev in range(4)]))
+    piece = jnp.roll(
+        jnp.concatenate(ring[::-1], axis=0), (lax.axis_index("tp") + 1) * ring[0].shape[0], axis=0
+    )
     gate_val = jnp.dot(piece, w_gate[0], preferred_element_type=jnp.float32)
     up_val = jnp.dot(piece, w_up[0], preferred_element_type=jnp.float32)
     hidden = (jax.nn.silu(gate_val) * up_val).astype(jnp.bfloat16)

time: 226 us -> 238 us (1.053)
  waiting for transfers between devices: 116 us -> 127 us
  local copies, waits for them, and re-layouts: 11.3 us -> 20 us
  matrix products: 29 us -> 20.5 us
    ppermute x0 -> x3, waiting for transfers between devices: none -> 51.5 us  [on_device(): lax.ppermute(ring[-1], 'tp', [(dev, (dev + 1) % 4) for dev in range(4)])]
    all_gather x1 -> x0, waiting for transfers between devices: 39.5 us -> none  [on_device(): piece = lax.all_gather(arrived, 'tp', axis=0, tiled=True)]
    dot_general x1, matrix products: 17.6 us -> 7.4 us  [on_device(): jnp.dot(piece, w_down[0], preferred_element_type=jnp.float32)]
    unnamed x14 -> x31, local copies, waits for them, and re-layouts: 1.92 us -> 9.93 us
    dot_general x0 -> x1, matrix products: none -> 5.96 us  [on_device(): up_val = jnp.dot(piece, w_up[0], preferred_element_type=jnp.float32)]
    dot_general x1, matrix products: 9.98 us -> 5.63 us  [on_device(): gate_val = jnp.dot(piece, w_gate[0], preferred_element_type=jnp.float32)]
  transfers between devices with their start and end apart: 5 -> 7, of which waited for: 3 -> 5; matrix products, arithmetic and copies ran while one was open for 5% -> 4% of each run, Pallas kernels for 0% -> 0%
where the time goes in v1:
time: 238 us; the launch traced here: 237 us
  waiting for transfers between devices  127 us (53%)
  blocking collectives  38.7 us (16%)
  matrix products  20.5 us (9%)
  local copies, waits for them, and re-layouts  20 us (8%)
  between operations  14.3 us (6%)
  starting transfers between devices  9.13 us (4%)
  other arithmetic  7.85 us (3%)
    ppermute x3, waiting for transfers between devices, on_device(): lax.ppermute(ring[-1], 'tp', [(dev, (dev + 1) % 4) for dev in range(4)])  51.5 us
    reduce_scatter x1, waiting for transfers between devices, on_device(): lax.psum_scatter(jnp.dot(piece, w_down[0], preferred_element_type=jnp.flo...  46.2 us
    all_to_all x1, blocking collectives, on_device(): lax.all_to_all(outgoing, 'ep', split_axis=0, concat_axis=1, tiled=True)  38.7 us
    all_to_all x1, waiting for transfers between devices, on_device(): lax.all_to_all(expert_out.reshape(n_ep, capacity, width), 'ep', split_axi...  29.3 us
    unnamed x31, local copies, waits for them, and re-layouts  9.93 us
    dot_general x1, matrix products, on_device(): jnp.dot(piece, w_down[0], preferred_element_type=jnp.float32)  7.4 us
    dot_general x1, matrix products, on_device(): up_val = jnp.dot(piece, w_up[0], preferred_element_type=jnp.float32)  5.96 us
    dot_general x1, matrix products, on_device(): gate_val = jnp.dot(piece, w_gate[0], preferred_element_type=jnp.float32)  5.63 us
  transfers between devices with their start and end apart: 7, of which 5 were waited for; matrix products, arithmetic and copies ran while one was open for 4% of the time, Pallas kernels for 0%

profile of v1, /device:TPU:0, one launch (start us, length us, event | category | flops | bytes accessed | tf_op | source)
XLA Modules:
  0.0 237.5 jit_solution(3511571550131706064)
XLA Ops:
  10.3 1.4 scatter_custom_fusion
  11.7 1.2 fusion.11
  12.9 1.2 fusion.13
  14.2 3.0 %gather_fusion = bf16[320,2048]{1,0:T(8,128)(2,1)} fusion(bf16[129,2048]{1,0:T(8,128)(2,1)S(1)} %concatenate.13, s32[1024]{0:T(1024)S(1)} %pad_clamp_fusion.1), kind=kCustom, calls=%fused_computation | custom fusion | bytes 2622720 | tf_op jit(solution)/shard_map/gather | solution.py:30
  17.3 38.7 %all_to_all.14 = bf16[8,40,2048]{2,1,0:T(8,128)(2,1)S(1)} all-to-all(bf16[8,40,2048]{2,1,0:T(8,128)(2,1)} %bitcast.34), channel_id=1, replica_groups=mesh['ep'=8,'tp'=4] {'ep'}, dimensions={0} | all-to-all | bytes 2621440 | tf_op jit(solution)/shard_map/all_to_all | solution.py:77
  56.0 17.0 %collective-permute-done.1 = bf16[320,2048]{1,0:T(8,128)(2,1)S(1)} collective-permute-done((bf16[320,2048]{1,0:T(8,128)(2,1)S(1)}, bf16[320,2048]{1,0:T(8,128)(2,1)S(1)}, u32[]{:S(2)}, u32[]{:S(2)}) %collective-permute-start.1) | collective-permute-done | bytes 1310752 | tf_op jit(solution)/shard_map/ppermute | solution.py:82
  73.0 1.1 copy-done.1
  74.1 17.1 %collective-permute-done.2 = bf16[320,2048]{1,0:T(8,128)(2,1)} collective-permute-done((bf16[320,2048]{1,0:T(8,128)(2,1)S(1)}, bf16[320,2048]{1,0:T(8,128)(2,1)}, u32[]{:S(2)}, u32[]{:S(2)}) %collective-permute-start.2) | collective-permute-done | bytes 1310752 | tf_op jit(solution)/shard_map/ppermute | solution.py:82
  91.2 17.3 %collective-permute-done.3 = bf16[320,2048]{1,0:T(8,128)(2,1)} collective-permute-done((bf16[320,2048]{1,0:T(8,128)(2,1)}, bf16[320,2048]{1,0:T(8,128)(2,1)}, u32[]{:S(2)}, u32[]{:S(2)}) %collective-permute-start.3) | collective-permute-done | bytes 1310752 | tf_op jit(solution)/shard_map/ppermute | solution.py:82
  108.6 1.4 constant_dynamic-update-slice_fusion.7
  110.0 1.5 constant_dynamic-update-slice_fusion.6
  111.7 1.5 constant_dynamic-update-slice_fusion.3
  113.2 1.6 constant_dynamic-update-slice_fusion.2
  115.6 5.6 %fusion.2 = f32[1280,896]{1,0:T(8,128)S(1)} fusion(bf16[2560,2048]{1,0:T(8,128)(2,1)S(1)} %constant_dynamic-update-slice_fusion, s32[]{:T(128)S(6)} %select_n.36, bf16[1,2048,896]{2,1,0:T(8,128)(2,1)S(1)} %copy-done.8), kind=kOutput, calls=%fused_computation.6 | convolution fusion | flops 4697620480 | bytes 13500420 | tf_op jit(solution)/shard_map/dot_general | solution.py:86
  121.3 6.0 %multiply_convert_fusion = bf16[1280,896]{1,0:T(8,128)(2,1)S(1)} fusion(f32[1280,896]{1,0:T(8,128)S(1)} %fusion.2, bf16[1,2048,896]{2,1,0:T(8,128)(2,1)S(1)} %copy-done.9, bf16[2560,2048]{1,0:T(8,128)(2,1)S(1)} %constant_dynamic-update-slice_fusion, s32[]{:T(128)S(6)} %select_n.36), kind=kOutput, calls=%fused_computation.8 | convolution fusion | flops 4704501760 | bytes 15794180 | tf_op jit(solution)/shard_map/dot_general | solution.py:87
  127.3 7.4 %convolution_convert_fusion = bf16[1280,2048]{1,0:T(8,128)(2,1)} fusion(bf16[1280,896]{1,0:T(8,128)(2,1)S(1)} %multiply_convert_fusion, bf16[1,896,2048]{2,1,0:T(8,128)(2,1)S(1)} %copy-done.10), kind=kOutput, calls=%fused_computation.3 | convolution fusion | flops 4700241920 | bytes 11206656 | tf_op jit(solution)/shard_map/dot_general | solution.py:91
  135.7 3.3 %collective-permute-start = (f32[2,256]{1,0:T(2,128)S(1)}, f32[2,256]{1,0:T(2,128)S(1)}, u32[]{:S(2)}, u32[]{:S(2)}) collective-permute-start(f32[2,256]{1,0:T(2,128)S(1)} %slice.36), channel_id=1, source_target_pairs={{0,4},{4,8},{8,12},{12,16},{16,20},{20,24},{24,28},{1,5},{5,9},{9,... | collective-permute-start | bytes 6152 | tf_op jit(solution)/shard_map/ppermute | solution.py:12
  139.0 46.2 %reduce-scatter.5.cloned.1.call-done = bf16[320,2048]{1,0:T(8,128)(2,1)} async-done(((bf16[1280,2048]{1,0:T(8,128)(2,1)}), bf16[320,2048]{1,0:T(8,128)(2,1)}) %reduce-scatter.5.cloned.1.call-update) | async-done | bytes 1310736 | tf_op jit(solution)/shard_map/reduce_scatter | solution.py:90
  185.2 5.5 %all-to-all-start.1 = ((bf16[8,40,2048]{2,1,0:T(8,128)(2,1)}), bf16[8,40,2048]{2,1,0:T(8,128)(2,1)S(1)}, u32[]{:S(2)}, u32[]{:S(2)}) async-start(bf16[8,40,2048]{2,1,0:T(8,128)(2,1)} %bitcast.35), calls=%async_computation.3 | async-start | bytes 2621440 | tf_op jit(solution)/shard_map/all_to_all | solution.py:96
  191.0 1.5 convolution_convert_fusion.1
  192.7 29.3 %all-to-all-done.1 = bf16[8,40,2048]{2,1,0:T(8,128)(2,1)S(1)} async-done(((bf16[8,40,2048]{2,1,0:T(8,128)(2,1)}), bf16[8,40,2048]{2,1,0:T(8,128)(2,1)S(1)}, u32[]{:S(2)}, u32[]{:S(2)}) %all-to-all-start.1) | async-done | bytes 1310752 | tf_op jit(solution)/shard_map/all_to_all | solution.py:96
  221.9 2.4 %gather_fusion.1 = bf16[256,2048]{1,0:T(8,128)(2,1)} fusion(bf16[320,2048]{1,0:T(8,128)(2,1)S(1)} %bitcast.30, s32[1024]{0:T(1024)S(1)} %pad_clamp_fusion), kind=kCustom, calls=%fused_computation.1 | custom fusion | bytes 2098176 | tf_op jit(solution)/shard_map/gather | solution.py:99
  224.3 2.4 reshape.85
  226.7 3.9 %multiply_reduce_fusion = bf16[128,2048]{1,0:T(8,128)(2,1)} fusion(f32[128,2,2048]{2,1,0:T(2,128)S(1)} %reshape.85, f32[128,2]{1,0:T(8,128)S(1)} %copy.18), kind=kLoop, calls=%fused_computation.13 | loop fusion | flops 786432 | bytes 2622464 | tf_op jit(solution)/shard_map/reduce_sum | solution.py:100
  (57 shorter events, 5.6 us)
Async XLA Ops:
  7.2 183.9 %copy-start = (bf16[256,2048]{1,0:T(8,128)(2,1)S(1)}, bf16[256,2048]{1,0:T(8,128)(2,1)}, u32[]{:S(2)}) copy-start(bf16[256,2048]{1,0:T(8,128)(2,1)} %param.16) | copy-start | bytes 3145732
  7.2 178.0 %reduce-scatter.5.cloned.1.call-start = ((), (), s32[]{:S(2)}) async-start(), calls=%async_computation.5 | async-start | bytes 6553600 | tf_op jit(solution)/shard_map/reduce_scatter | solution.py:90
  55.9 17.0 %collective-permute-start.1 = (bf16[320,2048]{1,0:T(8,128)(2,1)S(1)}, bf16[320,2048]{1,0:T(8,128)(2,1)S(1)}, u32[]{:S(2)}, u32[]{:S(2)}) collective-permute-start(bf16[320,2048]{1,0:T(8,128)(2,1)S(1)} %bitcast.31), channel_id=1, source_target_pairs={{0,1},{1,2},{2,3},{3,0},{4,5},{5,6},{6,7},{7,4},{8,9},{9,10},{10,1... | collective-permute-start | bytes 3932168 | tf_op jit(solution)/shard_map/ppermute | solution.py:82
  73.0 1.1 copy-start.1
  74.1 17.1 %collective-permute-start.2 = (bf16[320,2048]{1,0:T(8,128)(2,1)S(1)}, bf16[320,2048]{1,0:T(8,128)(2,1)}, u32[]{:S(2)}, u32[]{:S(2)}) collective-permute-start(bf16[320,2048]{1,0:T(8,128)(2,1)S(1)} %collective-permute-done.1), channel_id=1, source_target_pairs={{0,1},{1,2},{2,3},{3,0},{4,5},{5,6},{6,7},{7,4},{8,9},{9,10},{10,1... | collective-permute-start | bytes 3932168 | tf_op jit(solution)/shard_map/ppermute | solution.py:82
  91.2 17.3 %collective-permute-start.3 = (bf16[320,2048]{1,0:T(8,128)(2,1)}, bf16[320,2048]{1,0:T(8,128)(2,1)}, u32[]{:S(2)}, u32[]{:S(2)}) collective-permute-start(bf16[320,2048]{1,0:T(8,128)(2,1)} %collective-permute-done.2), channel_id=1, source_target_pairs={{0,1},{1,2},{2,3},{3,0},{4,5},{5,6},{6,7},{7,4},{8,9},{9,10},{10,1... | collective-permute-start | bytes 3932168 | tf_op jit(solution)/shard_map/ppermute | solution.py:82
  91.2 20.3 %copy-start.2 = (bf16[320,2048]{1,0:T(8,128)(2,1)S(1)}, bf16[320,2048]{1,0:T(8,128)(2,1)}, u32[]{:S(2)}) copy-start(bf16[320,2048]{1,0:T(8,128)(2,1)} %copy-done.1) | copy-start | bytes 3932164
  113.2 2.4 %copy-start.8 = (bf16[1,2048,896]{2,1,0:T(8,128)(2,1)S(1)}, bf16[1,2048,896]{2,1,0:T(8,128)(2,1)}, u32[]{:S(2)}) copy-start(bf16[1,2048,896]{2,1,0:T(8,128)(2,1)} %param.21) | copy-start | bytes 11010052
  115.6 5.6 %copy-start.9 = (bf16[1,2048,896]{2,1,0:T(8,128)(2,1)S(1)}, bf16[1,2048,896]{2,1,0:T(8,128)(2,1)}, u32[]{:S(2)}) copy-start(bf16[1,2048,896]{2,1,0:T(8,128)(2,1)} %param.22) | copy-start | bytes 11010052
  121.3 6.0 %copy-start.10 = (bf16[1,896,2048]{2,1,0:T(8,128)(2,1)S(1)}, bf16[1,896,2048]{2,1,0:T(8,128)(2,1)}, u32[]{:S(2)}) copy-start(bf16[1,896,2048]{2,1,0:T(8,128)(2,1)} %param.23) | copy-start | bytes 11010052
  134.7 0.9 copy-start.4
  134.7 1.0 copy-start.5
  134.7 56.3 %copy-start.6 = (f32[3,256]{1,0:T(4,128)S(1)}, f32[3,256]{1,0:T(4,128)}, u32[]{:S(2)}) copy-start(f32[3,256]{1,0:T(4,128)} %param.15) | copy-start | bytes 9220
  134.7 56.4 %copy-start.3 = (bf16[256,256]{1,0:T(8,128)(2,1)S(1)}, bf16[256,256]{1,0:T(8,128)(2,1)}, u32[]{:S(2)}) copy-start(bf16[256,256]{1,0:T(8,128)(2,1)} %param.13) | copy-start | bytes 393220
  135.6 56.9 %copy-start.7 = (f32[128,2]{0,1:T(2,128)S(1)}, f32[128,2]{0,1:T(2,128)}, u32[]{:S(2)}) copy-start(f32[128,2]{0,1:T(2,128)} %param.20) | copy-start | bytes 3076
  135.7 55.3 %collective-permute-start = (f32[2,256]{1,0:T(2,128)S(1)}, f32[2,256]{1,0:T(2,128)S(1)}, u32[]{:S(2)}, u32[]{:S(2)}) collective-permute-start(f32[2,256]{1,0:T(2,128)S(1)} %slice.36), channel_id=1, source_target_pairs={{0,4},{4,8},{8,12},{12,16},{16,20},{20,24},{24,28},{1,5},{5,9},{9,... | collective-permute-start | bytes 6152 | tf_op jit(solution)/shard_map/ppermute | solution.py:12
  185.2 36.7 %all-to-all-start.1 = ((bf16[8,40,2048]{2,1,0:T(8,128)(2,1)}), bf16[8,40,2048]{2,1,0:T(8,128)(2,1)S(1)}, u32[]{:S(2)}, u32[]{:S(2)}) async-start(bf16[8,40,2048]{2,1,0:T(8,128)(2,1)} %bitcast.35), calls=%async_computation.3 | async-start | bytes 2621440 | tf_op jit(solution)/shard_map/all_to_all | solution.py:96
  190.7 39.9 %reduce-scatter.3.cloned.1.call-start = ((), (), s32[]{:S(2)}) async-start(), calls=%async_computation.4 | async-start | bytes 1310720 | tf_op jit(solution)/shard_map/reduce_scatter | solution.py:57
Sparse Core Ops, SparseCore 0:
  134.8 50.3 reduce-scatter.4
  194.6 25.2 reduce-scatter.2
